TPU v7x, 128 devices: a whole 4x4x4 slice. The times are simulated.
128 devices in a mesh: ep: 128 (over z, y, x, core).
Axes of the slice: x: 4, y: 4, z: 4, core: 2. Of those that a mesh axis runs over, the one named last changes fastest.
Arguments:
- tokens: bfloat16 [2304, 2048], P('ep'), may hold values from -6 to 6
- attn_norm_gain: float32 [2048], replicated, may hold values from 0.1 to 1.9
- w_query: bfloat16 [2048, 512], replicated, may hold values from -0.125 to 0.125
- w_key: bfloat16 [2048, 128], replicated, may hold values from -0.125 to 0.125
- w_value: bfloat16 [2048, 128], replicated, may hold values from -0.125 to 0.125
- w_forget: bfloat16 [2048, 8], replicated, may hold values from -0.125 to 0.125
- forget_bias: float32 [8], replicated, may hold values from 0.5 to 4
- w_attn_out: bfloat16 [512, 2048], replicated, may hold values from -0.25 to 0.25
- cache_keys: bfloat16 [2304, 1024, 128], P('ep'), may hold values from -72 to 72
- cache_values: bfloat16 [2304, 1024, 128], P('ep'), may hold values from -6 to 6
- cache_logcum: float32 [2304, 8, 1024], P('ep'), as said below
- cache_lengths: int32 [2304], P('ep'), may hold values from 128 to 1024
- expert_norm_gain: float32 [2048], replicated, may hold values from 0.4 to 40
- expert_ids: int32 [2304, 6], P('ep'), may hold values from 0 to 127, all different within a row; in each aligned block of 18 rows (0 to 17, 18 to 35, ...) at most 2 rows name the same one
- expert_weights: float32 [2304, 6], P('ep'), may hold values from 0.1 to 1
- w_expert_gate: bfloat16 [128, 2048, 512], P('ep'), may hold values from -0.125 to 0.125
- w_expert_up: bfloat16 [128, 2048, 512], P('ep'), may hold values from -0.125 to 0.125
- w_expert_down: bfloat16 [128, 512, 2048], P('ep'), may hold values from -0.25 to 0.25
- w_dense_gate: bfloat16 [2048, 4096], P(None, 'ep'), may hold values from -0.125 to 0.125
- w_dense_up: bfloat16 [2048, 4096], P(None, 'ep'), may hold values from -2 to 2
- w_dense_down: bfloat16 [4096, 2048], P('ep'), may hold values from -0.09375 to 0.09375
- dense_norm_gain: float32 [4096], replicated, may hold values from 0.1 to 1.9
- branch_gate: float32 [2048], replicated, may hold values from -0.125 to 0.125
Outputs:
- result: bfloat16 [2304, 2048], P('ep')
Inputs may be any that keep to these rules, and one draw needn't show every extreme that they name: `cache_logcum`: along the positions of each sequence and head the values never rise. `expert_ids`: each row names 6 different experts; among the rows of one device no expert is named by more than 2 rows, and in every draw some device names some expert exactly 2 times.
All inputs are finite; a program needn't handle non-finite values.
Results may differ from a plain program's by a relative error of at most 0.012.
The roundings to bfloat16 on the way count: a program that leaves them out, or rounds other values in their place, can miss the bound.
Values may be sent and summed in bfloat16 or wider, within the bound.
A program may use at most 128 MiB of HBM per device.

v0:
```python
import jax
import jax.numpy as jnp
from jax import lax
from jax.sharding import PartitionSpec as P

HEADS = 8
KV_HEADS = 2
HEAD_DIM = 64
TOPK = 6
EPS = 1e-06
LIMIT = 7.0
ALPHA = 1.702


def normalize(values, gain):
    return values * lax.rsqrt(jnp.mean(values * values, axis=-1, keepdims=True) + EPS) * gain


def stored(values):
    return lax.optimization_barrier(values.astype(jnp.bfloat16))


def attend(
    query, key_new, value_new, log_forget, cache_keys, cache_values, cache_logcum, cache_lengths
):
    seqs, length = (cache_keys.shape[0], cache_keys.shape[1])
    group = HEADS // KV_HEADS
    scale = HEAD_DIM ** (-0.5)
    heads_q = query.reshape(seqs, KV_HEADS, group, HEAD_DIM)
    keys = cache_keys.reshape(seqs, length, KV_HEADS, HEAD_DIM)
    values = cache_values.reshape(seqs, length, KV_HEADS, HEAD_DIM)
    own_key = key_new.reshape(seqs, KV_HEADS, HEAD_DIM)
    own_value = value_new.astype(jnp.float32).reshape(seqs, KV_HEADS, 1, HEAD_DIM)
    last_index = jnp.broadcast_to((cache_lengths - 1)[:, None, None], (seqs, HEADS, 1))
    carried = jnp.take_along_axis(cache_logcum, last_index, axis=2)[:, :, 0] + log_forget
    offset = (carried[:, :, None] - cache_logcum).reshape(seqs, KV_HEADS, group, length)
    scores = (
        jnp.einsum("skgd,slkd->skgl", heads_q, keys, preferred_element_type=jnp.float32) * scale
        + offset
    )
    live = jnp.arange(length, dtype=jnp.int32)[None, :] < cache_lengths[:, None]
    scores = jnp.where(live[:, None, None, :], scores, -jnp.inf)
    own = jnp.einsum("skgd,skd->skg", heads_q, own_key, preferred_element_type=jnp.float32) * scale
    top = jnp.maximum(jnp.max(scores, axis=-1), own)
    expo = jnp.exp(scores - top[..., None])
    own_expo = jnp.exp(own - top)
    total = jnp.sum(expo, axis=-1) + own_expo
    weights = (expo / total[..., None]).astype(jnp.bfloat16)
    own_weight = stored(own_expo / total).astype(jnp.float32)
    out = jnp.einsum("skgl,slkd->skgd", weights, values, preferred_element_type=jnp.float32)
    out = out + own_weight[..., None] * own_value
    return out.reshape(seqs, HEADS * HEAD_DIM).astype(jnp.bfloat16)


def expert_unit(rows, gate_w, up_w, down_w):
    gate = jnp.minimum(jnp.dot(rows, gate_w, preferred_element_type=jnp.float32), LIMIT)
    up = jnp.clip(jnp.dot(rows, up_w, preferred_element_type=jnp.float32), -LIMIT, LIMIT)
    act = ((up + 1.0) * gate * jax.nn.sigmoid(gate * ALPHA)).astype(jnp.bfloat16)
    return jnp.dot(act, down_w, preferred_element_type=jnp.float32).astype(jnp.bfloat16)


def shards(
    tokens,
    attn_norm_gain,
    w_query,
    w_key,
    w_value,
    w_forget,
    forget_bias,
    w_attn_out,
    cache_keys,
    cache_values,
    cache_logcum,
    cache_lengths,
    expert_norm_gain,
    expert_ids,
    expert_weights,
    w_expert_gate,
    w_expert_up,
    w_expert_down,
    w_dense_gate,
    w_dense_up,
    w_dense_down,
    dense_norm_gain,
    branch_gate,
):
    seqs, width = (tokens.shape[0], tokens.shape[1])
    normed = normalize(tokens.astype(jnp.float32), attn_norm_gain).astype(jnp.bfloat16)
    query = jnp.dot(normed, w_query, preferred_element_type=jnp.float32).astype(jnp.bfloat16)
    key_new = jnp.dot(normed, w_key, preferred_element_type=jnp.float32).astype(jnp.bfloat16)
    value_new = jnp.dot(normed, w_value, preferred_element_type=jnp.float32).astype(jnp.bfloat16)
    log_forget = jax.nn.log_sigmoid(
        jnp.dot(normed, w_forget, preferred_element_type=jnp.float32) + forget_bias
    )
    attended = attend(
        query, key_new, value_new, log_forget, cache_keys, cache_values, cache_logcum, cache_lengths
    )
    mixed = stored(
        tokens.astype(jnp.float32)
        + jnp.dot(attended, w_attn_out, preferred_element_type=jnp.float32)
    )
    routed_in = normalize(mixed.astype(jnp.float32), expert_norm_gain).astype(jnp.bfloat16)
    devices = lax.axis_size("ep")
    experts = devices * w_expert_gate.shape[0]
    capacity = max(2, 2 * seqs * TOPK // experts)
    flat_ids = expert_ids.reshape(-1)
    member = (flat_ids[:, None] == jnp.arange(experts, dtype=jnp.int32)[None, :]).astype(jnp.int32)
    slot = jnp.sum(jnp.cumsum(member, axis=0) * member, axis=1) - 1
    target = flat_ids * capacity + slot
    placement = (
        target[:, None] == jnp.arange(experts * capacity, dtype=jnp.int32)[None, :]
    ).astype(jnp.float32)
    per_token = jnp.sum(placement.reshape(seqs, TOPK, experts * capacity), axis=1).astype(
        jnp.bfloat16
    )
    outgoing = jnp.einsum("sc,sd->cd", per_token, routed_in, preferred_element_type=jnp.float32)
    outgoing = outgoing.astype(jnp.bfloat16).reshape(experts, capacity, width)
    arrived = lax.all_to_all(outgoing, "ep", split_axis=0, concat_axis=0, tiled=True)
    count = arrived.shape[1]
    answer = expert_unit(
        arrived.reshape(-1, width), w_expert_gate[0], w_expert_up[0], w_expert_down[0]
    )
    returned = lax.all_to_all(
        answer.reshape(devices, count, width), "ep", split_axis=0, concat_axis=0, tiled=True
    )
    picked = jnp.dot(
        placement.astype(jnp.bfloat16),
        returned.reshape(experts * capacity, width),
        preferred_element_type=jnp.float32,
    )
    routed = jnp.sum(expert_weights[:, :, None] * picked.reshape(seqs, TOPK, width), axis=1)
    piece = lax.all_gather(routed_in, "ep", axis=0, tiled=True)
    gate_dense = jnp.dot(piece, w_dense_gate, preferred_element_type=jnp.float32)
    up_dense = jnp.dot(piece, w_dense_up, preferred_element_type=jnp.float32)
    units = (jax.nn.silu(gate_dense) * up_dense).astype(jnp.bfloat16)
    own_units = lax.all_to_all(units, "ep", split_axis=0, concat_axis=1, tiled=True).astype(
        jnp.float32
    )
    unit_scale = lax.rsqrt(jnp.mean(own_units * own_units, axis=1, keepdims=True) + EPS)
    hidden = (own_units * unit_scale * dense_norm_gain).astype(jnp.bfloat16)
    dense = jnp.dot(
        hidden,
        lax.all_gather(w_dense_down, "ep", axis=0, tiled=True),
        preferred_element_type=jnp.float32,
    )
    branch_scale = jax.nn.sigmoid(
        jnp.sum(routed_in.astype(jnp.float32) * branch_gate, axis=1, keepdims=True)
    )
    return (mixed.astype(jnp.float32) + routed + branch_scale * dense).astype(jnp.bfloat16)


def solution(mesh):
    in_specs = (
        P("ep", None),
        P(),
        P(),
        P(),
        P(),
        P(),
        P(),
        P(),
        P("ep", None, None),
        P("ep", None, None),
        P("ep", None, None),
        P("ep"),
        P(),
        P("ep", None),
        P("ep", None),
        P("ep", None, None),
        P("ep", None, None),
        P("ep", None, None),
        P(None, "ep"),
        P(None, "ep"),
        P("ep", None),
        P(),
        P(),
    )
    out_specs = P("ep", None)
    return jax.shard_map(shards, mesh=mesh, in_specs=in_specs, out_specs=out_specs, check_vma=False)
```

profile of v0, /device:TPU:1, one launch (start us, length us, event | category | flops | bytes accessed | tf_op | source)
XLA Modules:
  0.0 229.7 jit_solution(16532619259781696633)
XLA Ops:
  6.5 0.8 broadcast_add_fusion.1
  7.3 0.7 broadcast_compare_fusion
  8.0 0.7 iota_compare_fusion.2
  8.8 0.1 copy.49
  8.9 0.1 reshape.290
  9.0 5.7 %gather_fusion = f32[144]{0:T(256)S(1)} fusion(f32[18,8,1024]{2,1,0:T(8,128)} %param.33, s32[144]{0:T(256)S(1)} %reshape.290), kind=kCustom, calls=%fused_computation | custom fusion | bytes 2880 | tf_op jit(solution)/shard_map/jit(take_along_axis)/gather | solution.py:35
  14.7 0.1 gather.7
  14.9 0.1 fusion.48
  15.1 0.2 fusion.62
  15.3 0.1 copy.51
  15.4 0.9 broadcast_subtract_fusion
  16.3 1.2 reshape.279
  17.5 2.0 convolution_convert_fusion.2
  19.6 0.1 reshape.277
  19.7 6.7 %copy.48 = bf16[18,1024,128]{1,2,0:T(8,128)(2,1)} copy(bf16[18,1024,128]{2,1,0:T(8,128)(2,1)} %param.31) | data formatting | bytes 9437184 | tf_op args[8]
  26.4 0.2 convolution_convert_fusion.4
  26.6 0.1 reshape.304
  26.7 0.2 fusion.81
  26.9 3.3 %fusion.80 = (f32[18,2,4]{2,1,0:T(2,128)S(1)}, f32[18,2,4,1024]{3,2,1,0:T(4,128)S(1)}) fusion(f32[18,2,4,1024]{3,2,1,0:T(4,128)S(1)} %reshape.279, bf16[18,2,4,64]{3,2,1,0:T(4,128)(2,1)S(1)} %reshape.277, bf16[18,1024,2,64]{1,3,2,0:T(8,128)(2,1)} %bitcast.60, pred[18,1024]{1,0:T(8,128)(4,1)S(1)} %iota_compare_fusion.2), kind=kOutput, calls=%fused_computation.112 | convolution fusion | flops 19464048 | bytes 5935680 | tf_op jit(solution)/shard_map/skgd,slkd->skgl/dot_general | solution.py:38
  30.2 0.4 fusion.41
  30.6 0.2 fusion.32
  30.9 0.1 reshape.286
  31.0 6.6 %copy.52 = bf16[18,1024,128]{1,2,0:T(8,128)(2,1)} copy(bf16[18,1024,128]{2,1,0:T(8,128)(2,1)} %param.32) | data formatting | bytes 9437184 | tf_op args[9]
  37.6 3.7 %fusion.31 = bf16[18,2,4,64]{3,2,1,0:T(4,128)(2,1)S(1)} fusion(bf16[18,1024,2,64]{1,3,2,0:T(8,128)(2,1)} %bitcast.61, f32[18,2,4,1024]{3,2,1,0:T(4,128)S(1)} %get-tuple-element.12, f32[18,2,4]{2,1,0:T(2,128)S(1)} %get-tuple-element.8, f32[18,2,4]{2,1,0:T(2,128)S(1)} %multiply_maximum_fusion, f32[18,2,64]{2,1,0:T(2,128)S(1)} %reshape.286, ...), kind=kOutput, calls=%fused_computation.30 | convolution fusion | flops 19344384 | bytes 5337792 | tf_op jit(solution)/shard_map/skgl,slkd->skgd/dot_general | solution.py:50
  41.4 0.1 convert_element_type.130
  41.5 2.0 fusion.2
  43.4 0.1 fusion.51
  43.6 0.9 multiply_reduce_fusion
  44.5 0.7 all-gather.4.cloned.1.call-update
  45.3 0.1 copy.54
  45.4 0.1 eq.49
  45.4 0.1 fusion.59
  45.5 0.2 reduce_window_sum.11
  45.7 0.2 select_reduce_fusion
  45.9 0.1 sub.35
  46.0 0.1 convert_reduce_fusion
  46.1 0.5 convolution_convert_fusion.1
  46.6 1.5 reshape.282
  48.2 31.4 %all_to_all.23 = bf16[128,2,2048]{2,1,0:T(2,128)(2,1)S(1)} all-to-all(bf16[128,2,2048]{2,1,0:T(2,128)(2,1)} %reshape.282), channel_id=1, replica_groups=mesh['ep'=128] {'ep'}, dimensions={0} | all-to-all | bytes 2097152 | tf_op jit(solution)/shard_map/all_to_all | solution.py:118
  79.6 1.2 reshape.283
  80.8 3.5 %fusion.16 = f32[256,512]{1,0:T(8,128)} fusion(bf16[256,2048]{1,0:T(8,128)(2,1)} %reshape.283, bf16[1,2048,512]{2,1,0:T(8,128)(2,1)} %param.38), kind=kOutput, calls=%fused_computation.24 | convolution fusion | flops 537001984 | bytes 3670016 | tf_op jit(solution)/shard_map/dot_general | solution.py:56
  84.3 4.1 %convolution_convert_fusion = bf16[256,2048]{1,0:T(8,128)(2,1)} fusion(bf16[1,512,2048]{2,1,0:T(8,128)(2,1)S(1)} %copy-done, f32[256,512]{1,0:T(8,128)} %fusion.16, bf16[256,2048]{1,0:T(8,128)(2,1)S(1)} %copy-done.5, bf16[1,2048,512]{2,1,0:T(8,128)(2,1)} %param.39), kind=kOutput, calls=%fused_computation.3 | convolution fusion | flops 1075445760 | bytes 6815744 | tf_op jit(solution)/shard_map/dot_general | solution.py:59
  88.4 2.6 %reshape.284 = bf16[128,2,2048]{2,1,0:T(2,128)(2,1)} reshape(bf16[256,2048]{1,0:T(8,128)(2,1)} %convolution_convert_fusion) | data formatting | bytes 2097152 | tf_op jit(solution)/shard_map/reshape | solution.py:124
  90.9 4.5 %all-to-all-start.1 = ((bf16[128,2,2048]{2,1,0:T(2,128)(2,1)}), bf16[128,2,2048]{2,1,0:T(2,128)(2,1)S(1)}, u32[]{:S(2)}, u32[]{:S(2)}) async-start(bf16[128,2,2048]{2,1,0:T(2,128)(2,1)} %reshape.284), calls=%async_computation.1 | async-start | bytes 2097152 | tf_op jit(solution)/shard_map/all_to_all | solution.py:123
  95.5 0.1 copy.53
  95.6 21.0 %all-to-all-done.1 = bf16[128,2,2048]{2,1,0:T(2,128)(2,1)S(1)} async-done(((bf16[128,2,2048]{2,1,0:T(2,128)(2,1)}), bf16[128,2,2048]{2,1,0:T(2,128)(2,1)S(1)}, u32[]{:S(2)}, u32[]{:S(2)}) %all-to-all-start.1) | async-done | bytes 1048608 | tf_op jit(solution)/shard_map/all_to_all | solution.py:123
  116.6 0.4 reshape.302
  117.0 14.3 %all-gather.6.cloned.1.call-done = bf16[128,18,2048]{2,1,0:T(8,128)(2,1)} async-done(((bf16[1,18,2048]{2,1,0:T(8,128)(2,1)}), bf16[128,18,2048]{2,1,0:T(8,128)(2,1)}) %all-gather.6.cloned.1.call-update) | async-done | bytes 9437200 | tf_op jit(solution)/shard_map/all_gather | solution.py:132
  131.3 14.1 %reshape.299 = bf16[2304,2048]{1,0:T(8,128)(2,1)} reshape(bf16[128,18,2048]{2,1,0:T(8,128)(2,1)} %all-gather.6.cloned.1.call-done) | data formatting | bytes 18874368
  145.4 6.8 %fusion.82 = f32[2304,32]{0,1:T(8,128)S(1)} fusion(bf16[2304,2048]{1,0:T(8,128)(2,1)} %reshape.299, bf16[2048,32]{0,1:T(8,128)(2,1)S(1)} %copy-done.8), kind=kOutput, calls=%fused_computation.114 | convolution fusion | flops 301989888 | bytes 9863168 | tf_op jit(solution)/shard_map/dot_general | solution.py:133
  152.2 2.9 %fusion = bf16[2304,32]{0,1:T(8,128)(2,1)S(1)} fusion(bf16[2304,2048]{1,0:T(8,128)(2,1)S(1)} %copy-done.3, bf16[2048,32]{0,1:T(8,128)(2,1)S(1)} %copy-done.9, f32[2304,32]{0,1:T(8,128)S(1)} %fusion.82), kind=kOutput, calls=%fused_computation.2 | convolution fusion | flops 302432256 | bytes 10010624 | tf_op jit(solution)/shard_map/dot_general | solution.py:134
  155.1 2.5 %all_to_all.18 = bf16[128,18,32]{1,0,2:T(8,128)(2,1)S(1)} reshape(bf16[2304,32]{0,1:T(8,128)(2,1)S(1)} %fusion) | data formatting | bytes 294912 | tf_op jit(solution)/shard_map/all_to_all | solution.py:136
  157.7 1.5 copy.56
  159.2 1.2 reshape.306
  160.4 5.8 %all-to-all-start.2 = ((bf16[128,2,288]{2,1,0:T(2,128)(2,1)}), bf16[128,2,288]{2,1,0:T(2,128)(2,1)S(1)}, u32[]{:S(2)}, u32[]{:S(2)}) async-start(bf16[128,2,288]{2,1,0:T(2,128)(2,1)} %reshape.306), calls=%async_computation.2 | async-start | bytes 393216 | tf_op jit(solution)/shard_map/all_to_all | solution.py:136
  166.2 0.6 fusion.10
  166.8 10.8 %all-to-all-done.2 = bf16[128,2,288]{2,1,0:T(2,128)(2,1)S(1)} async-done(((bf16[128,2,288]{2,1,0:T(2,128)(2,1)}), bf16[128,2,288]{2,1,0:T(2,128)(2,1)S(1)}, u32[]{:S(2)}, u32[]{:S(2)}) %all-to-all-start.2) | async-done | bytes 147488 | tf_op jit(solution)/shard_map/all_to_all | solution.py:136
  177.6 0.5 reshape.307
  178.1 0.1 convert_bitcast_fusion
  178.2 0.2 copy.57
  178.5 0.5 reshape.287
  179.0 0.4 fusion.9
  179.4 34.6 %all-gather.4.cloned.1.call-done = bf16[4096,2048]{1,0:T(8,128)(2,1)} async-done(((bf16[32,2048]{1,0:T(8,128)(2,1)}), bf16[4096,2048]{1,0:T(8,128)(2,1)}) %all-gather.4.cloned.1.call-update) | async-done | bytes 16777232 | tf_op jit(solution)/shard_map/all_gather | solution.py:143
  214.0 8.9 %fusion.3 = bf16[18,2048]{1,0:T(8,128)(2,1)} fusion(bf16[4096,2048]{1,0:T(8,128)(2,1)} %all-gather.4.cloned.1.call-done, f32[18,2048]{1,0:T(8,128)S(1)} %fusion.10, bf16[18,2048]{1,0:T(8,128)(2,1)S(1)} %fusion.2, f32[18,4096]{1,0:T(8,128)S(1)} %reshape.287, f32[4096]{0:T(1024)S(1)} %copy-done.11, f32[18]{0:T(128)S(1)} %add_rsqrt_fusion, ...), kind=kOutput, calls=%fused_computation.10 | convolution fusion | flops 302395392 | bytes 17383568 | tf_op jit(solution)/shard_map/dot_general | solution.py:141
  (54 shorter events, 0.4 us)
Async XLA Ops:
  6.5 77.8 %copy-start = (bf16[1,512,2048]{2,1,0:T(8,128)(2,1)S(1)}, bf16[1,512,2048]{2,1,0:T(8,128)(2,1)}, u32[]{:S(2)}) copy-start(bf16[1,512,2048]{2,1,0:T(8,128)(2,1)} %param.40) | copy-start | bytes 6291460
  6.5 124.8 %all-gather.6.cloned.1.call-start = ((), (), s32[]{:S(2)}) async-start(), calls=%async_computation.4 | async-start | bytes 12681216 | tf_op jit(solution)/shard_map/all_gather | solution.py:132
  9.0 5.9 %copy-start.4 = (bf16[18,2048]{1,0:T(8,128)(2,1)S(1)}, bf16[18,2048]{1,0:T(8,128)(2,1)}, u32[]{:S(2)}) copy-start(bf16[18,2048]{1,0:T(8,128)(2,1)} %param.23) | copy-start | bytes 221188
  9.0 6.0 %copy-start.10 = (f32[2048]{0:T(1024)S(1)}, f32[2048]{0:T(1024)}, u32[]{:S(2)}) copy-start(f32[2048]{0:T(1024)} %param.24) | copy-start | bytes 24580
  9.0 6.0 %copy-start.16 = (bf16[2048,8]{0,1:T(8,128)(2,1)S(1)}, bf16[2048,8]{0,1:T(8,128)(2,1)}, u32[]{:S(2)}) copy-start(bf16[2048,8]{0,1:T(8,128)(2,1)} %param.28) | copy-start | bytes 98308
  9.0 6.0 %copy-start.17 = (f32[8]{0:T(128)S(1)}, f32[8]{0:T(128)}, u32[]{:S(2)}) copy-start(f32[8]{0:T(128)} %param.29) | copy-start | bytes 100
  9.0 6.3 %copy-start.2 = (f32[18,8,1024]{2,1,0:T(8,128)S(1)}, f32[18,8,1024]{2,1,0:T(8,128)}, u32[]{:S(2)}) copy-start(f32[18,8,1024]{2,1,0:T(8,128)} %param.33) | copy-start | bytes 1769476
  19.7 6.7 %copy-start.6 = (bf16[2048,128]{1,0:T(8,128)(2,1)S(1)}, bf16[2048,128]{1,0:T(8,128)(2,1)}, u32[]{:S(2)}) copy-start(bf16[2048,128]{1,0:T(8,128)(2,1)} %param.26) | copy-start | bytes 1572868
  26.9 3.7 %copy-start.7 = (bf16[2048,128]{1,0:T(8,128)(2,1)S(1)}, bf16[2048,128]{1,0:T(8,128)(2,1)}, u32[]{:S(2)}) copy-start(bf16[2048,128]{1,0:T(8,128)(2,1)} %param.27) | copy-start | bytes 1572868
  41.3 2.3 copy-start.12
  41.3 2.3 copy-start.13
  41.3 3.9 %copy-start.14 = (s32[18,6]{0,1:T(8,128)S(1)}, s32[18,6]{0,1:T(8,128)}, u32[]{:S(2)}) copy-start(s32[18,6]{0,1:T(8,128)} %param.36) | copy-start | bytes 1300
  44.5 169.5 %all-gather.4.cloned.1.call-start = ((), (), s32[]{:S(2)}) async-start(), calls=%async_computation.3 | async-start | bytes 16908288 | tf_op jit(solution)/shard_map/all_gather | solution.py:143
  80.8 3.5 %copy-start.5 = (bf16[256,2048]{1,0:T(8,128)(2,1)S(1)}, bf16[256,2048]{1,0:T(8,128)(2,1)}, u32[]{:S(2)}) copy-start(bf16[256,2048]{1,0:T(8,128)(2,1)} %reshape.283) | copy-start | bytes 3145732
  88.4 7.1 %copy-start.15 = (f32[18,6]{0,1:T(8,128)S(1)}, f32[18,6]{0,1:T(8,128)}, u32[]{:S(2)}) copy-start(f32[18,6]{0,1:T(8,128)} %param.37) | copy-start | bytes 1300
  90.9 25.6 %all-to-all-start.1 = ((bf16[128,2,2048]{2,1,0:T(2,128)(2,1)}), bf16[128,2,2048]{2,1,0:T(2,128)(2,1)S(1)}, u32[]{:S(2)}, u32[]{:S(2)}) async-start(bf16[128,2,2048]{2,1,0:T(2,128)(2,1)} %reshape.284), calls=%async_computation.1 | async-start | bytes 2097152 | tf_op jit(solution)/shard_map/all_to_all | solution.py:123
  117.0 28.4 %copy-start.8 = (bf16[2048,32]{0,1:T(8,128)(2,1)S(1)}, bf16[2048,32]{0,1:T(8,128)(2,1)}, u32[]{:S(2)}) copy-start(bf16[2048,32]{0,1:T(8,128)(2,1)} %param.41) | copy-start | bytes 393220
  145.4 6.8 %copy-start.3 = (bf16[2304,2048]{1,0:T(8,128)(2,1)S(1)}, bf16[2304,2048]{1,0:T(8,128)(2,1)}, u32[]{:S(2)}) copy-start(bf16[2304,2048]{1,0:T(8,128)(2,1)} %reshape.299) | copy-start | bytes 28311556
  145.4 6.8 %copy-start.9 = (bf16[2048,32]{0,1:T(8,128)(2,1)S(1)}, bf16[2048,32]{0,1:T(8,128)(2,1)}, u32[]{:S(2)}) copy-start(bf16[2048,32]{0,1:T(8,128)(2,1)} %param.42) | copy-start | bytes 393220
  160.4 17.2 %all-to-all-start.2 = ((bf16[128,2,288]{2,1,0:T(2,128)(2,1)}), bf16[128,2,288]{2,1,0:T(2,128)(2,1)S(1)}, u32[]{:S(2)}, u32[]{:S(2)}) async-start(bf16[128,2,288]{2,1,0:T(2,128)(2,1)} %reshape.306), calls=%async_computation.2 | async-start | bytes 393216 | tf_op jit(solution)/shard_map/all_to_all | solution.py:136
  178.2 35.8 %copy-start.11 = (f32[4096]{0:T(1024)S(1)}, f32[4096]{0:T(1024)}, u32[]{:S(2)}) copy-start(f32[4096]{0:T(1024)} %param.44) | copy-start | bytes 49156
  214.0 8.9 %copy-start.1 = (bf16[1,512,2048]{2,1,0:T(8,128)(2,1)S(1)}, bf16[1,512,2048]{2,1,0:T(8,128)(2,1)}, u32[]{:S(2)}) copy-start(bf16[1,512,2048]{2,1,0:T(8,128)(2,1)} %param.40) | copy-start | bytes 6291460
Sparse Core Ops, SparseCore 0:
  44.6 86.6 all-gather.5
  134.5 79.4 all-gather.3
where the time goes:
time: 231 us; the launch traced here: 230 us
  waiting for transfers between devices  81.3 us (35%)
  local copies, waits for them, and re-layouts  47.9 us (21%)
  matrix products  39.1 us (17%)
  blocking collectives  31.4 us (14%)
  between operations  13.8 us (6%)
  starting transfers between devices  10.4 us (5%)
  other arithmetic  5.76 us (2%)
    all_gather x1, waiting for transfers between devices, shards(): lax.all_gather(w_dense_down, 'ep', axis=0, tiled=True)  34.6 us
    all_to_all x1, blocking collectives, shards(): lax.all_to_all(outgoing, 'ep', split_axis=0, concat_axis=0, tiled=True)  31.4 us
    unnamed x45, local copies, waits for them, and re-layouts  29.5 us
    all_to_all x1, waiting for transfers between devices, shards(): lax.all_to_all(answer.reshape(devices, count, width), 'ep', split_axis=0,...  21 us
    all_gather x1, waiting for transfers between devices, shards(): piece = lax.all_gather(routed_in, 'ep', axis=0, tiled=True)  14.3 us
    all_to_all x1, waiting for transfers between devices, shards(): lax.all_to_all(units, 'ep', split_axis=0, concat_axis=1, tiled=True)  10.8 us
    dot_general x1, matrix products, shards(): jnp.dot(hidden, lax.all_gather(w_dense_down, 'ep', axis=0, tiled=True), p...  8.89 us
    dot_general x1, matrix products, shards(): jnp.dot(piece, w_dense_gate, preferred_element_type=jnp.float32)  6.78 us
  transfers between devices with their start and end apart: 4, of which 4 were waited for; matrix products, arithmetic and copies ran while one was open for 19% of the time, Pallas kernels for 0%

commit v1 on v0

--- a/solution.py
+++ b/solution.py
@@ -140,7 +140,9 @@
     hidden = (own_units * unit_scale * dense_norm_gain).astype(jnp.bfloat16)
     dense = jnp.dot(
         hidden,
-        lax.all_gather(w_dense_down, "ep", axis=0, tiled=True),
+        jnp.concatenate(
+            lax.all_to_all(jnp.stack([w_dense_down] * lax.axis_size("ep")), "ep", 0, 0), axis=0
+        ),
         preferred_element_type=jnp.float32,
     )
     branch_scale = jax.nn.sigmoid(

time: 231 us -> 441 us (1.91)
  the two profiles are of different devices: /device:TPU:1 before, /device:TPU:84 now
where the time goes in v1:
time: 441 us; the launch traced here: 440 us
  waiting for transfers between devices  269 us (61%)
  local copies, waits for them, and re-layouts  52.2 us (12%)
  blocking collectives  38.7 us (9%)
  matrix products  38.4 us (9%)
  starting transfers between devices  22 us (5%)
  between operations  13.8 us (3%)
  other arithmetic  5.66 us (1%)
    all_to_all x1, waiting for transfers between devices, shards(): lax.all_to_all(jnp.stack([w_dense_down] * lax.axis_size('ep')), 'ep', 0, 0)  237 us
    all_gather x1, waiting for transfers between devices, shards(): piece = lax.all_gather(routed_in, 'ep', axis=0, tiled=True)  31.8 us
    unnamed x47, local copies, waits for them, and re-layouts  28.8 us
    all_to_all x1, blocking collectives, shards(): lax.all_to_all(outgoing, 'ep', split_axis=0, concat_axis=0, tiled=True)  24.6 us
    all_to_all x1, blocking collectives, shards(): lax.all_to_all(units, 'ep', split_axis=0, concat_axis=1, tiled=True)  14.2 us
    all_to_all x1, starting transfers between devices, shards(): lax.all_to_all(jnp.stack([w_dense_down] * lax.axis_size('ep')), 'ep', 0, 0)  11.5 us
    all_to_all x1, starting transfers between devices, shards(): lax.all_to_all(answer.reshape(devices, count, width), 'ep', split_axis=0,...  10.4 us
  transfers between devices with their start and end apart: 3, of which 2 were waited for; matrix products, arithmetic and copies ran while one was open for 10% of the time, Pallas kernels for 0%

profile of v1, /device:TPU:84, one launch (start us, length us, event | category | flops | bytes accessed | tf_op | source)
XLA Modules:
  0.0 440.1 jit_solution(17654018630801836910)
XLA Ops:
  6.5 0.8 broadcast_add_fusion.1
  7.3 0.7 broadcast_compare_fusion
  8.0 0.7 iota_compare_fusion.2
  8.8 0.1 copy.52
  8.9 0.1 reshape.301
  9.0 5.4 %gather_fusion = f32[144]{0:T(256)S(1)} fusion(f32[18,8,1024]{2,1,0:T(8,128)} %param.33, s32[144]{0:T(256)S(1)} %reshape.301), kind=kCustom, calls=%fused_computation | custom fusion | bytes 2880 | tf_op jit(solution)/shard_map/jit(take_along_axis)/gather | solution.py:35
  14.4 0.1 gather.7
  14.5 0.1 copy.53
  14.6 0.1 fusion.55
  14.8 0.2 fusion.67
  15.0 0.1 copy.54
  15.1 0.9 broadcast_subtract_fusion
  16.0 1.2 reshape.291
  17.3 2.0 convolution_convert_fusion.2
  19.3 0.1 reshape.289
  19.4 6.7 %copy.51 = bf16[18,1024,128]{1,2,0:T(8,128)(2,1)} copy(bf16[18,1024,128]{2,1,0:T(8,128)(2,1)} %param.31) | data formatting | bytes 9437184 | tf_op args[8]
  26.1 0.2 convolution_convert_fusion.4
  26.4 0.1 reshape.316
  26.4 0.2 fusion.86
  26.6 3.3 fusion.85
  29.9 0.4 fusion.48
  30.4 0.2 fusion.35
  30.6 0.1 reshape.298
  30.7 6.6 %copy.55 = bf16[18,1024,128]{1,2,0:T(8,128)(2,1)} copy(bf16[18,1024,128]{2,1,0:T(8,128)(2,1)} %param.32) | data formatting | bytes 9437184 | tf_op args[9]
  37.4 3.7 fusion.34
  41.1 0.1 convert_element_type.127
  41.2 2.0 fusion.4
  43.2 0.1 fusion.58
  43.4 0.9 multiply_reduce_fusion
  44.2 0.0 all-gather.3.cloned.1.call-update
  44.2 0.1 copy.57
  44.3 0.1 eq.49
  44.4 0.1 fusion.64
  44.5 0.2 reduce_window_sum.11
  44.7 0.2 select_reduce_fusion
  44.9 0.1 sub.35
  45.0 0.1 convert_reduce_fusion
  45.1 0.5 convolution_convert_fusion.1
  45.6 1.5 reshape.294
  47.1 24.6 %all_to_all.28 = bf16[128,2,2048]{2,1,0:T(2,128)(2,1)S(1)} all-to-all(bf16[128,2,2048]{2,1,0:T(2,128)(2,1)} %reshape.294), channel_id=1, replica_groups=mesh['ep'=128] {'ep'}, dimensions={0} | all-to-all | bytes 2097152 | tf_op jit(solution)/shard_map/all_to_all | solution.py:118
  71.7 1.2 reshape.295
  73.0 3.5 fusion.19
  76.4 4.1 convolution_convert_fusion
  80.5 2.5 reshape.296
  83.1 10.4 %all-to-all-start.1 = ((bf16[128,2,2048]{2,1,0:T(2,128)(2,1)}), bf16[128,2,2048]{2,1,0:T(2,128)(2,1)S(1)}, u32[]{:S(2)}, u32[]{:S(2)}) async-start(bf16[128,2,2048]{2,1,0:T(2,128)(2,1)} %reshape.296), calls=%async_computation.1 | async-start | bytes 2097152 | tf_op jit(solution)/shard_map/all_to_all | solution.py:123
  93.5 31.8 %all-gather.3.cloned.1.call-done = bf16[128,18,2048]{2,1,0:T(8,128)(2,1)} async-done(((bf16[1,18,2048]{2,1,0:T(8,128)(2,1)}), bf16[128,18,2048]{2,1,0:T(8,128)(2,1)}) %all-gather.3.cloned.1.call-update) | async-done | bytes 9437200 | tf_op jit(solution)/shard_map/all_gather | solution.py:132
  125.4 14.1 %reshape.310 = bf16[2304,2048]{1,0:T(8,128)(2,1)} reshape(bf16[128,18,2048]{2,1,0:T(8,128)(2,1)} %all-gather.3.cloned.1.call-done) | data formatting | bytes 18874368
  139.5 6.7 %fusion.87 = f32[2304,32]{0,1:T(8,128)S(1)} fusion(bf16[2304,2048]{1,0:T(8,128)(2,1)} %reshape.310, bf16[2048,32]{0,1:T(8,128)(2,1)S(1)} %copy-done.8), kind=kOutput, calls=%fused_computation.117 | convolution fusion | flops 301989888 | bytes 9863168 | tf_op jit(solution)/shard_map/dot_general | solution.py:133
  146.2 0.0 copy-done.3
  146.2 2.9 fusion
  149.1 2.5 all_to_all.21
  151.6 1.5 copy.59
  153.2 0.5 reshape.318
  153.7 14.2 %all_to_all.29 = bf16[128,2,288]{2,1,0:T(2,128)(2,1)S(1)} all-to-all(bf16[128,2,288]{2,1,0:T(2,128)(2,1)S(1)} %reshape.318), channel_id=1, replica_groups=mesh['ep'=128] {'ep'}, dimensions={0} | all-to-all | bytes 294912 | tf_op jit(solution)/shard_map/all_to_all | solution.py:136
  167.9 6.0 %stack.2 = bf16[128,32,2048]{2,1,0:T(8,128)(2,1)} broadcast(bf16[32,2048]{1,0:T(8,128)(2,1)S(1)} %copy-done.10), dimensions={1,2} | broadcast | bytes 16908288 | tf_op jit(solution)/shard_map/stack | solution.py:144
  173.9 11.5 %all-to-all-start.3 = ((bf16[128,32,2048]{2,1,0:T(8,128)(2,1)}), bf16[128,32,2048]{2,1,0:T(8,128)(2,1)}, u32[]{:S(2)}, u32[]{:S(2)}) async-start(bf16[128,32,2048]{2,1,0:T(8,128)(2,1)} %stack.2), calls=%async_computation.3 | async-start | bytes 33554432 | tf_op jit(solution)/shard_map/all_to_all | solution.py:144
  185.5 0.1 copy.56
  185.6 0.1 mul.187
  185.6 0.4 reshape.313
  186.1 0.6 fusion.13
  186.7 0.5 reshape.319
  187.2 0.4 fusion.10
  187.6 237.5 %all-to-all-done.3 = bf16[128,32,2048]{2,1,0:T(8,128)(2,1)} async-done(((bf16[128,32,2048]{2,1,0:T(8,128)(2,1)}), bf16[128,32,2048]{2,1,0:T(8,128)(2,1)}, u32[]{:S(2)}, u32[]{:S(2)}) %all-to-all-start.3) | async-done | bytes 16777248 | tf_op jit(solution)/shard_map/all_to_all | solution.py:144
  425.1 8.2 %fusion.3 = bf16[18,2048]{1,0:T(8,128)(2,1)} fusion(bf16[128,32,2048]{2,1,0:T(8,128)(2,1)} %all-to-all-done.3, bf16[128,18,32]{2,1,0:T(8,128)(2,1)S(1)} %reshape.319, f32[128,32]{1,0:T(8,128)S(1)} %mul.187, f32[18]{0:T(128)S(1)} %add_rsqrt_fusion, f32[18,2048]{1,0:T(8,128)S(1)} %fusion.13, bf16[18,2048]{1,0:T(8,128)(2,1)S(1)} %fusion.4, ...), kind=kOutput, calls=%fused_computation.10 | convolution fusion | flops 302469120 | bytes 17236112 | tf_op jit(solution)/shard_map/dot_general | solution.py:141
  (53 shorter events, 0.2 us)
Async XLA Ops:
  6.5 69.9 %copy-start = (bf16[1,512,2048]{2,1,0:T(8,128)(2,1)S(1)}, bf16[1,512,2048]{2,1,0:T(8,128)(2,1)}, u32[]{:S(2)}) copy-start(bf16[1,512,2048]{2,1,0:T(8,128)(2,1)} %param.40) | copy-start | bytes 6291460
  6.5 118.8 %all-gather.3.cloned.1.call-start = ((), (), s32[]{:S(2)}) async-start(), calls=%async_computation.4 | async-start | bytes 12681216 | tf_op jit(solution)/shard_map/all_gather | solution.py:132
  9.0 5.6 %copy-start.4 = (bf16[18,2048]{1,0:T(8,128)(2,1)S(1)}, bf16[18,2048]{1,0:T(8,128)(2,1)}, u32[]{:S(2)}) copy-start(bf16[18,2048]{1,0:T(8,128)(2,1)} %param.23) | copy-start | bytes 221188
  9.0 5.8 %copy-start.11 = (f32[2048]{0:T(1024)S(1)}, f32[2048]{0:T(1024)}, u32[]{:S(2)}) copy-start(f32[2048]{0:T(1024)} %param.24) | copy-start | bytes 24580
  9.0 5.8 %copy-start.17 = (bf16[2048,8]{0,1:T(8,128)(2,1)S(1)}, bf16[2048,8]{0,1:T(8,128)(2,1)}, u32[]{:S(2)}) copy-start(bf16[2048,8]{0,1:T(8,128)(2,1)} %param.28) | copy-start | bytes 98308
  9.0 5.8 %copy-start.18 = (f32[8]{0:T(128)S(1)}, f32[8]{0:T(128)}, u32[]{:S(2)}) copy-start(f32[8]{0:T(128)} %param.29) | copy-start | bytes 100
  9.0 6.1 %copy-start.2 = (f32[18,8,1024]{2,1,0:T(8,128)S(1)}, f32[18,8,1024]{2,1,0:T(8,128)}, u32[]{:S(2)}) copy-start(f32[18,8,1024]{2,1,0:T(8,128)} %param.33) | copy-start | bytes 1769476
  19.4 6.7 %copy-start.6 = (bf16[2048,128]{1,0:T(8,128)(2,1)S(1)}, bf16[2048,128]{1,0:T(8,128)(2,1)}, u32[]{:S(2)}) copy-start(bf16[2048,128]{1,0:T(8,128)(2,1)} %param.26) | copy-start | bytes 1572868
  26.6 3.7 copy-start.7
  41.1 2.3 copy-start.12
  41.1 2.3 copy-start.14
  41.1 3.2 copy-start.15
  73.0 3.5 copy-start.5
  83.1 70.6 %all-to-all-start.1 = ((bf16[128,2,2048]{2,1,0:T(2,128)(2,1)}), bf16[128,2,2048]{2,1,0:T(2,128)(2,1)S(1)}, u32[]{:S(2)}, u32[]{:S(2)}) async-start(bf16[128,2,2048]{2,1,0:T(2,128)(2,1)} %reshape.296), calls=%async_computation.1 | async-start | bytes 2097152 | tf_op jit(solution)/shard_map/all_to_all | solution.py:123
  93.5 45.9 %copy-start.8 = (bf16[2048,32]{0,1:T(8,128)(2,1)S(1)}, bf16[2048,32]{0,1:T(8,128)(2,1)}, u32[]{:S(2)}) copy-start(bf16[2048,32]{0,1:T(8,128)(2,1)} %param.41) | copy-start | bytes 393220
  139.4 6.7 %copy-start.3 = (bf16[2304,2048]{1,0:T(8,128)(2,1)S(1)}, bf16[2304,2048]{1,0:T(8,128)(2,1)}, u32[]{:S(2)}) copy-start(bf16[2304,2048]{1,0:T(8,128)(2,1)} %reshape.310) | copy-start | bytes 28311556
  139.4 6.8 %copy-start.9 = (bf16[2048,32]{0,1:T(8,128)(2,1)S(1)}, bf16[2048,32]{0,1:T(8,128)(2,1)}, u32[]{:S(2)}) copy-start(bf16[2048,32]{0,1:T(8,128)(2,1)} %param.42) | copy-start | bytes 393220
  149.1 18.8 %copy-start.10 = (bf16[32,2048]{1,0:T(8,128)(2,1)S(1)}, bf16[32,2048]{1,0:T(8,128)(2,1)}, u32[]{:S(2)}) copy-start(bf16[32,2048]{1,0:T(8,128)(2,1)} %param.43) | copy-start | bytes 393220
  173.9 11.5 %copy-start.16 = (f32[18,6]{0,1:T(8,128)S(1)}, f32[18,6]{0,1:T(8,128)}, u32[]{:S(2)}) copy-start(f32[18,6]{0,1:T(8,128)} %param.37) | copy-start | bytes 1300
  173.9 11.6 %copy-start.13 = (f32[4096]{0:T(1024)S(1)}, f32[4096]{0:T(1024)}, u32[]{:S(2)}) copy-start(f32[4096]{0:T(1024)} %param.44) | copy-start | bytes 49156
  173.9 251.2 %all-to-all-start.3 = ((bf16[128,32,2048]{2,1,0:T(8,128)(2,1)}), bf16[128,32,2048]{2,1,0:T(8,128)(2,1)}, u32[]{:S(2)}, u32[]{:S(2)}) async-start(bf16[128,32,2048]{2,1,0:T(8,128)(2,1)} %stack.2), calls=%async_computation.3 | async-start | bytes 33554432 | tf_op jit(solution)/shard_map/all_to_all | solution.py:144
  425.1 8.2 %copy-start.1 = (bf16[1,512,2048]{2,1,0:T(8,128)(2,1)S(1)}, bf16[1,512,2048]{2,1,0:T(8,128)(2,1)}, u32[]{:S(2)}) copy-start(bf16[1,512,2048]{2,1,0:T(8,128)(2,1)} %param.40) | copy-start | bytes 6291460
Sparse Core Ops, SparseCore 0:
  44.4 80.9 all-gather.2
